TPU v7x, 32 devices: a whole 2x2x4 slice. The times are simulated.
32 devices in a mesh: sp: 8 (over z, y), tp: 4 (over x, core).
Axes of the slice: x: 2, y: 2, z: 4, core: 2. Of those that a mesh axis runs over, the one named last changes fastest.
Arguments:
- stream: bfloat16 [2048, 2048], P('sp', 'tp'), may hold values from -6 to 6
- norm_gain: float32 [2, 2048], replicated, may hold values from 0.1 to 1.9
- w_value: bfloat16 [2, 2048, 1024], P(None, 'sp', 'tp'), may hold values from -0.125 to 0.125
- w_gate: bfloat16 [2, 2048, 1024], P(None, 'sp', 'tp'), may hold values from -0.125 to 0.125
- conv_taps: float32 [2, 128, 1024], P(None, None, 'tp'), as said below
- channel_gain: float32 [2, 1024], P(None, 'tp'), may hold values from 0.1 to 1.9
- w_out: bfloat16 [2, 1024, 2048], P(None, 'tp', 'sp'), may hold values from -0.1875 to 0.1875
Outputs:
- result: bfloat16 [2048, 2048], P('sp', 'tp')
Inputs may be any that keep to these rules, and one draw needn't show every extreme that they name: `conv_taps`: taps of each block of 128 consecutive channels share a scale factor of its own.
All inputs are finite; a program needn't handle non-finite values.
Results may differ from a plain program's by a relative error of at most 0.012.
Values may be sent and summed in bfloat16 or wider, within the bound.
A program may use at most 64 MiB of HBM per device.

v0:
```python
import jax
import jax.numpy as jnp
from jax import lax
from jax.sharding import PartitionSpec as P

C = 1024
LAYERS = 2


def from_behind(value, axis, steps):
    count = lax.axis_size(axis)
    initial, last = (max(0, -steps), min(count, count - steps))
    return lax.ppermute(value, axis, [(source, source + steps) for source in range(initial, last)])


def shards(stream, norm_gain, w_value, w_gate, conv_taps, channel_gain, w_out):
    x = stream
    tokens_here = stream.shape[0]
    local_ch = w_value.shape[2]
    taps = conv_taps.shape[1]
    for layer in range(LAYERS):
        whole = lax.all_gather(x, "tp", axis=1, tiled=True).astype(jnp.float32)
        normed = (
            whole
            * lax.rsqrt(jnp.mean(whole * whole, axis=1, keepdims=True) + 1e-06)
            * norm_gain[layer]
        ).astype(jnp.bfloat16)
        value_whole, gate_whole = (
            lax.all_gather(w_value[layer], "sp", axis=0, tiled=True),
            lax.all_gather(w_gate[layer], "sp", axis=0, tiled=True),
        )
        value = jnp.dot(normed, value_whole, preferred_element_type=jnp.float32)
        gate = jnp.dot(normed, gate_whole, preferred_element_type=jnp.float32)
        glu = (value * jax.nn.sigmoid(gate)).astype(jnp.bfloat16)
        before = from_behind(glu[tokens_here - taps :], "sp", 1)
        padded = jnp.concatenate([before[1:], glu], axis=0).astype(jnp.float32)
        conv = lax.conv_general_dilated(
            padded[None],
            conv_taps[layer][:, None, :],
            (1,),
            "VALID",
            dimension_numbers=("NWC", "WIO", "NWC"),
            feature_group_count=local_ch,
            precision=lax.Precision.HIGHEST,
        )[0]
        mean = lax.psum(jnp.sum(conv, axis=1, keepdims=True), "tp") / C
        centred = conv - mean
        spread = lax.psum(jnp.sum(centred * centred, axis=1, keepdims=True), "tp") / C
        act = jax.nn.silu(centred * lax.rsqrt(spread + 1e-05) * channel_gain[layer]).astype(
            jnp.bfloat16
        )
        out_whole = lax.all_gather(w_out[layer], "sp", axis=1, tiled=True)
        terms = jnp.dot(act, out_whole, preferred_element_type=jnp.float32)
        branch = lax.psum_scatter(terms, "tp", scatter_dimension=1, tiled=True)
        x = (x.astype(jnp.float32) + branch).astype(jnp.bfloat16)
    return x


def solution(mesh):
    return jax.shard_map(
        shards,
        mesh=mesh,
        in_specs=(
            P("sp", "tp"),
            P(),
            P(None, "sp", "tp"),
            P(None, "sp", "tp"),
            P(None, None, "tp"),
            P(None, "tp"),
            P(None, "tp", "sp"),
        ),
        out_specs=P("sp", "tp"),
        check_vma=False,
    )
```

profile of v0, /device:TPU:0, one launch (start us, length us, event | category | flops | bytes accessed | tf_op | source)
XLA Modules:
  0.0 370.0 jit_solution(6867189528916284857)
XLA Ops:
  12.7 15.7 %all-gather.15.cloned.1.call-done = bf16[256,2048]{1,0:T(8,128)(2,1)} async-done(((bf16[256,512]{1,0:T(8,128)(2,1)}), bf16[256,2048]{1,0:T(8,128)(2,1)}) %all-gather.15.cloned.1.call-update) | async-done | bytes 1048592 | tf_op jit(solution)/shard_map/all_gather | solution.py:22
  30.0 40.8 %all-gather.19.cloned.1.call-done = bf16[1,2048,256]{2,1,0:T(8,128)(2,1)} async-done(((bf16[1,256,256]{2,1,0:T(8,128)(2,1)}), bf16[1,2048,256]{2,1,0:T(8,128)(2,1)}) %all-gather.19.cloned.1.call-update) | async-done | bytes 1048592 | tf_op jit(solution)/shard_map/all_gather | solution.py:29
  70.8 2.0 fusion.24
  72.8 39.1 %all-gather.21.cloned.1.call-done = bf16[1,2048,256]{2,1,0:T(8,128)(2,1)} async-done(((bf16[1,256,256]{2,1,0:T(8,128)(2,1)}), bf16[1,2048,256]{2,1,0:T(8,128)(2,1)}) %all-gather.21.cloned.1.call-update) | async-done | bytes 1048592 | tf_op jit(solution)/shard_map/all_gather | solution.py:30
  113.7 2.5 collective-permute-start
  116.2 1.9 collective-permute-done
  118.1 4.8 %fusion.50 = (f32[256]{0:T(256)S(1)}, f32[1,256,256]{2,0,1:T(1,128)S(1)}) fusion(f32[1,128,256]{2,1,0:T(8,128)S(1)} %get-tuple-element.6, bf16[1,383,256]{2,1,0:T(8,128)(2,1)S(1)} %maximum_bitcast_fusion), kind=kOutput, calls=%fused_computation.70 | convolution fusion | flops 100728576 | bytes 590336 | tf_op jit(solution)/shard_map/conv_general_dilated | solution.py:37
  123.0 5.7 %psum.28 = f32[256,1]{0,1:T(1,128)S(1)} all-reduce(f32[256,1]{0,1:T(1,128)S(1)} %bitcast.72), channel_id=1, replica_groups=mesh['sp'=8,'tp'=4] {'tp'}, use_global_device_ids=true, to_apply=%region_2.0 | all-reduce | flops 256 | bytes 2048 | tf_op jit(solution)/shard_map/psum | solution.py:46
  128.8 7.0 %psum.29 = f32[256,1]{0,1:T(1,128)S(1)} all-reduce(f32[256,1]{0,1:T(1,128)S(1)} %bitcast.68), channel_id=1, replica_groups=mesh['sp'=8,'tp'=4] {'tp'}, use_global_device_ids=true, to_apply=%region_4.0 | all-reduce | flops 256 | bytes 2048 | tf_op jit(solution)/shard_map/psum | solution.py:48
  135.8 16.2 %all-gather.23.cloned.1.call-done = bf16[1,256,2048]{2,1,0:T(8,128)(2,1)} async-done(((bf16[1,256,256]{2,1,0:T(8,128)(2,1)}), bf16[1,256,2048]{2,1,0:T(8,128)(2,1)}) %all-gather.23.cloned.1.call-update) | async-done | bytes 1048592 | tf_op jit(solution)/shard_map/all_gather | solution.py:52
  152.0 3.1 fusion.21
  155.2 30.3 %reduce-scatter.3.cloned.1.call-done = f32[256,512]{1,0:T(8,128)} async-done(((f32[256,2048]{1,0:T(8,128)}), f32[256,512]{1,0:T(8,128)}) %reduce-scatter.3.cloned.1.call-update) | async-done | bytes 524304 | tf_op jit(solution)/shard_map/reduce_scatter | solution.py:54
  189.6 14.6 %all-gather.17.cloned.1.call-done = bf16[256,2048]{1,0:T(8,128)(2,1)} async-done(((bf16[256,512]{1,0:T(8,128)(2,1)}), bf16[256,2048]{1,0:T(8,128)(2,1)}) %all-gather.17.cloned.1.call-update) | async-done | bytes 1048592 | tf_op jit(solution)/shard_map/all_gather | solution.py:22
  205.8 40.8 %all-gather.25.cloned.1.call-done = bf16[1,2048,256]{2,1,0:T(8,128)(2,1)} async-done(((bf16[1,256,256]{2,1,0:T(8,128)(2,1)}), bf16[1,2048,256]{2,1,0:T(8,128)(2,1)}) %all-gather.25.cloned.1.call-update) | async-done | bytes 1048592 | tf_op jit(solution)/shard_map/all_gather | solution.py:29
  246.6 2.0 fusion.19
  248.6 39.1 %all-gather.27.cloned.1.call-done = bf16[1,2048,256]{2,1,0:T(8,128)(2,1)} async-done(((bf16[1,256,256]{2,1,0:T(8,128)(2,1)}), bf16[1,2048,256]{2,1,0:T(8,128)(2,1)}) %all-gather.27.cloned.1.call-update) | async-done | bytes 1048592 | tf_op jit(solution)/shard_map/all_gather | solution.py:30
  289.5 2.5 collective-permute-start.1
  292.0 1.9 collective-permute-done.1
  293.9 4.8 %fusion.51 = (f32[256]{0:T(256)S(1)}, f32[1,256,256]{2,0,1:T(1,128)S(1)}) fusion(f32[1,128,256]{2,1,0:T(8,128)S(1)} %get-tuple-element.5, bf16[1,383,256]{2,1,0:T(8,128)(2,1)S(1)} %maximum_bitcast_fusion.1), kind=kOutput, calls=%fused_computation.71 | convolution fusion | flops 100728576 | bytes 590336 | tf_op jit(solution)/shard_map/conv_general_dilated | solution.py:37
  298.8 5.7 %psum.30 = f32[256,1]{0,1:T(1,128)S(1)} all-reduce(f32[256,1]{0,1:T(1,128)S(1)} %bitcast.73), channel_id=1, replica_groups=mesh['sp'=8,'tp'=4] {'tp'}, use_global_device_ids=true, to_apply=%region_8.9 | all-reduce | flops 256 | bytes 2048 | tf_op jit(solution)/shard_map/psum | solution.py:46
  304.6 7.0 %psum.31 = f32[256,1]{0,1:T(1,128)S(1)} all-reduce(f32[256,1]{0,1:T(1,128)S(1)} %bitcast.69), channel_id=1, replica_groups=mesh['sp'=8,'tp'=4] {'tp'}, use_global_device_ids=true, to_apply=%region_10.11 | all-reduce | flops 256 | bytes 2048 | tf_op jit(solution)/shard_map/psum | solution.py:48
  311.6 16.3 %all-gather.29.cloned.1.call-done = bf16[1,256,2048]{2,1,0:T(8,128)(2,1)} async-done(((bf16[1,256,256]{2,1,0:T(8,128)(2,1)}), bf16[1,256,2048]{2,1,0:T(8,128)(2,1)}) %all-gather.29.cloned.1.call-update) | async-done | bytes 1048592 | tf_op jit(solution)/shard_map/all_gather | solution.py:52
  327.9 3.1 fusion.16
  331.1 30.3 %reduce-scatter.5.cloned.1.call-done = f32[256,512]{1,0:T(8,128)} async-done(((f32[256,2048]{1,0:T(8,128)}), f32[256,512]{1,0:T(8,128)}) %reduce-scatter.5.cloned.1.call-update) | async-done | bytes 524304 | tf_op jit(solution)/shard_map/reduce_scatter | solution.py:54
  (60 shorter events, 19.2 us)
Async XLA Ops:
  6.5 6.1 %copy-start.5 = (f32[2,2048]{1,0:T(2,128)S(1)}, f32[2,2048]{1,0:T(2,128)}, u32[]{:S(2)}) copy-start(f32[2,2048]{1,0:T(2,128)} %param.8) | copy-start | bytes 49156
  6.5 6.1 %copy-start.4 = (f32[2,128,256]{2,1,0:T(8,128)S(1)}, f32[2,128,256]{2,1,0:T(8,128)}, u32[]{:S(2)}) copy-start(f32[2,128,256]{2,1,0:T(8,128)} %param.11) | copy-start | bytes 786436
  6.5 21.8 %all-gather.15.cloned.1.call-start = ((), (), s32[]{:S(2)}) async-start(), calls=%async_computation.2 | async-start | bytes 1310720 | tf_op jit(solution)/shard_map/all_gather | solution.py:22
  7.3 63.5 %all-gather.19.cloned.1.call-start = ((), (), s32[]{:S(2)}) async-start(), calls=%async_computation.6 | async-start | bytes 1179648 | tf_op jit(solution)/shard_map/all_gather | solution.py:29
  9.0 102.9 %all-gather.21.cloned.1.call-start = ((), (), s32[]{:S(2)}) async-start(), calls=%async_computation.7 | async-start | bytes 1179648 | tf_op jit(solution)/shard_map/all_gather | solution.py:30
  10.8 141.2 %all-gather.23.cloned.1.call-start = ((), (), s32[]{:S(2)}) async-start(), calls=%async_computation.8 | async-start | bytes 1179648 | tf_op jit(solution)/shard_map/all_gather | solution.py:52
  12.6 172.9 %reduce-scatter.3.cloned.1.call-start = ((), (), s32[]{:S(2)}) async-start(), calls=%async_computation.3 | async-start | bytes 2621440 | tf_op jit(solution)/shard_map/reduce_scatter | solution.py:54
  28.4 83.6 %copy-start.1 = (bf16[256,2048]{1,0:T(8,128)(2,1)S(1)}, bf16[256,2048]{1,0:T(8,128)(2,1)}, u32[]{:S(2)}) copy-start(bf16[256,2048]{1,0:T(8,128)(2,1)} %all-gather.15.cloned.1.call-done) | copy-start | bytes 3145732
  72.8 43.4 %copy-start.6 = (f32[2,256]{1,0:T(2,128)S(1)}, f32[2,256]{1,0:T(2,128)}, u32[]{:S(2)}) copy-start(f32[2,256]{1,0:T(2,128)} %param.12) | copy-start | bytes 6148
  113.7 4.4 %collective-permute-start = (bf16[128,256]{1,0:T(8,128)(2,1)S(1)}, bf16[128,256]{1,0:T(8,128)(2,1)S(1)}, u32[]{:S(2)}, u32[]{:S(2)}) collective-permute-start(bf16[128,256]{1,0:T(8,128)(2,1)S(1)} %slice.64), channel_id=1, source_target_pairs={{0,4},{4,8},{8,12},{12,16},{16,20},{20,24},{24,28},{1,5},{5,9},{9,... | collective-permute-start | bytes 196616 | tf_op jit(solution)/shard_map/ppermute | solution.py:13
  152.0 33.5 %copy-start.3 = (bf16[256,512]{1,0:T(8,128)(2,1)S(1)}, bf16[256,512]{1,0:T(8,128)(2,1)}, u32[]{:S(2)}) copy-start(bf16[256,512]{1,0:T(8,128)(2,1)} %param.7) | copy-start | bytes 786436
  155.1 49.0 %all-gather.17.cloned.1.call-start = ((), (), s32[]{:S(2)}) async-start(), calls=%async_computation.4 | async-start | bytes 1310720 | tf_op jit(solution)/shard_map/all_gather | solution.py:22
  187.3 59.3 %all-gather.25.cloned.1.call-start = ((), (), s32[]{:S(2)}) async-start(), calls=%async_computation.9 | async-start | bytes 1179648 | tf_op jit(solution)/shard_map/all_gather | solution.py:29
  188.0 99.7 %all-gather.27.cloned.1.call-start = ((), (), s32[]{:S(2)}) async-start(), calls=%async_computation.10 | async-start | bytes 1179648 | tf_op jit(solution)/shard_map/all_gather | solution.py:30
  188.8 139.1 %all-gather.29.cloned.1.call-start = ((), (), s32[]{:S(2)}) async-start(), calls=%async_computation.11 | async-start | bytes 1179648 | tf_op jit(solution)/shard_map/all_gather | solution.py:52
  189.5 171.9 %reduce-scatter.5.cloned.1.call-start = ((), (), s32[]{:S(2)}) async-start(), calls=%async_computation.5 | async-start | bytes 2621440 | tf_op jit(solution)/shard_map/reduce_scatter | solution.py:54
  204.1 83.6 %copy-start.2 = (bf16[256,2048]{1,0:T(8,128)(2,1)S(1)}, bf16[256,2048]{1,0:T(8,128)(2,1)}, u32[]{:S(2)}) copy-start(bf16[256,2048]{1,0:T(8,128)(2,1)} %all-gather.17.cloned.1.call-done) | copy-start | bytes 3145732
  289.5 4.4 %collective-permute-start.1 = (bf16[128,256]{1,0:T(8,128)(2,1)S(1)}, bf16[128,256]{1,0:T(8,128)(2,1)S(1)}, u32[]{:S(2)}, u32[]{:S(2)}) collective-permute-start(bf16[128,256]{1,0:T(8,128)(2,1)S(1)} %slice.66), channel_id=1, source_target_pairs={{0,4},{4,8},{8,12},{12,16},{16,20},{20,24},{24,28},{1,5},{5,9},{9,... | collective-permute-start | bytes 196616 | tf_op jit(solution)/shard_map/ppermute | solution.py:13
  327.9 33.5 %copy-start = (bf16[256,512]{1,0:T(8,128)(2,1)S(1)}, bf16[256,512]{1,0:T(8,128)(2,1)}, u32[]{:S(2)}) copy-start(bf16[256,512]{1,0:T(8,128)(2,1)} %add_convert_fusion.1) | copy-start | bytes 786436
Sparse Core Ops, SparseCore 0:
  8.9 19.4 all-gather.14
  30.5 40.2 all-gather.18
  72.9 38.9 all-gather.20
  113.8 38.0 all-gather.22
  155.2 30.1 reduce-scatter.2
  187.4 16.6 all-gather.16
  206.3 40.2 all-gather.24
  248.7 38.9 all-gather.26
  289.8 38.0 all-gather.28
  331.2 30.1 reduce-scatter.4
where the time goes:
time: 371 us; the launch traced here: 370 us
  waiting for transfers between devices  290 us (78%)
  blocking collectives  25.3 us (7%)
  matrix products  23.4 us (6%)
  between operations  13.7 us (4%)
  other arithmetic  7.31 us (2%)
  starting transfers between devices  5.32 us (1%)
  local copies, waits for them, and re-layouts  5.19 us (1%)
    all_gather x2, waiting for transfers between devices, shards(): lax.all_gather(w_value[layer], 'sp', axis=0, tiled=True)  81.7 us
    all_gather x2, waiting for transfers between devices, shards(): lax.all_gather(w_gate[layer], 'sp', axis=0, tiled=True)  78.2 us
    reduce_scatter x2, waiting for transfers between devices, shards(): branch = lax.psum_scatter(terms, 'tp', scatter_dimension=1, tiled=True)  60.6 us
    all_gather x2, waiting for transfers between devices, shards(): out_whole = lax.all_gather(w_out[layer], 'sp', axis=1, tiled=True)  32.5 us
    all_gather x2, waiting for transfers between devices, shards(): whole = lax.all_gather(x, 'tp', axis=1, tiled=True).astype(jnp.float32)  30.3 us
    psum x2, blocking collectives, shards(): lax.psum(jnp.sum(centred * centred, axis=1, keepdims=True), 'tp') / C  14 us
    psum x2, blocking collectives, shards(): mean = lax.psum(jnp.sum(conv, axis=1, keepdims=True), 'tp') / C  11.3 us
    conv_general_dilated x2, matrix products, shards(): lax.conv_general_dilated(padded[None], conv_taps[layer][:, None, :], (1,)...  9.67 us
  transfers between devices with their start and end apart: 12, of which 12 were waited for; matrix products, arithmetic and copies ran while one was open for 7% of the time, Pallas kernels for 0%

commit v1 on v0

--- a/solution.py
+++ b/solution.py
@@ -19,7 +19,7 @@
     local_ch = w_value.shape[2]
     taps = conv_taps.shape[1]
     for layer in range(LAYERS):
-        whole = lax.all_gather(x, "tp", axis=1, tiled=True).astype(jnp.float32)
+        whole = jnp.concatenate(lax.all_gather(x, "tp"), axis=1).astype(jnp.float32)
         normed = (
             whole
             * lax.rsqrt(jnp.mean(whole * whole, axis=1, keepdims=True) + 1e-06)

time: 371 us -> 371 us (level)
  waiting for transfers between devices: 290 us -> 283 us
  local copies, waits for them, and re-layouts: 5.19 us -> 9.19 us
  other arithmetic: 7.31 us -> 11.1 us
    all_gather x2, waiting for transfers between devices: 81.7 us -> 73.8 us  [shards(): lax.all_gather(w_value[layer], 'sp', axis=0, tiled=True)]
    convert_element_type x0 -> x4, other arithmetic: none -> 6.38 us  [the longest x2 5.69 us: shards(): whole = jnp.concatenate(lax.all_gather(x, 'tp'), axis=1).astype(jnp.float32)]
    convert_element_type x0 -> x2, local copies, waits for them, and re-layouts: none -> 4.01 us  [shards(): whole = jnp.concatenate(lax.all_gather(x, 'tp'), axis=1).astype(jnp.float32)]
  transfers between devices with their start and end apart: 12 -> 12, of which waited for: 12 -> 12; matrix products, arithmetic and copies ran while one was open for 7% -> 9% of each run, Pallas kernels for 0% -> 0%
where the time goes in v1:
time: 371 us; the launch traced here: 370 us
  waiting for transfers between devices  283 us (76%)
  blocking collectives  25.3 us (7%)
  matrix products  22.7 us (6%)
  between operations  13.7 us (4%)
  other arithmetic  11.1 us (3%)
  local copies, waits for them, and re-layouts  9.19 us (2%)
  starting transfers between devices  5.32 us (1%)
    all_gather x2, waiting for transfers between devices, shards(): lax.all_gather(w_gate[layer], 'sp', axis=0, tiled=True)  78.9 us
    all_gather x2, waiting for transfers between devices, shards(): lax.all_gather(w_value[layer], 'sp', axis=0, tiled=True)  73.8 us
    reduce_scatter x2, waiting for transfers between devices, shards(): branch = lax.psum_scatter(terms, 'tp', scatter_dimension=1, tiled=True)  60.6 us
    all_gather x2, waiting for transfers between devices, shards(): out_whole = lax.all_gather(w_out[layer], 'sp', axis=1, tiled=True)  32.5 us
    all_gather x2, waiting for transfers between devices, shards(): whole = jnp.concatenate(lax.all_gather(x, 'tp'), axis=1).astype(jnp.float32)  30.3 us
    psum x2, blocking collectives, shards(): lax.psum(jnp.sum(centred * centred, axis=1, keepdims=True), 'tp') / C  14 us
    psum x2, blocking collectives, shards(): mean = lax.psum(jnp.sum(conv, axis=1, keepdims=True), 'tp') / C  11.3 us
    conv_general_dilated x2, matrix products, shards(): lax.conv_general_dilated(padded[None], conv_taps[layer][:, None, :], (1,)...  9.67 us
  transfers between devices with their start and end apart: 12, of which 12 were waited for; matrix products, arithmetic and copies ran while one was open for 9% of the time, Pallas kernels for 0%

profile of v1, /device:TPU:0, one launch (start us, length us, event | category | flops | bytes accessed | tf_op | source)
XLA Modules:
  0.0 370.0 jit_solution(12283603965417174620)
XLA Ops:
  12.7 15.7 %all-gather.17.cloned.1.call-done = bf16[1024,512]{1,0:T(8,128)(2,1)} async-done(((bf16[256,512]{1,0:T(8,128)(2,1)}), bf16[1024,512]{1,0:T(8,128)(2,1)}) %all-gather.17.cloned.1.call-update) | async-done | bytes 1048592 | tf_op jit(solution)/shard_map/all_gather | solution.py:22
  28.3 2.8 convert_bitcast_fusion
  31.2 2.0 copy.17
  33.9 36.9 %all-gather.19.cloned.1.call-done = bf16[1,2048,256]{2,1,0:T(8,128)(2,1)} async-done(((bf16[1,256,256]{2,1,0:T(8,128)(2,1)}), bf16[1,2048,256]{2,1,0:T(8,128)(2,1)}) %all-gather.19.cloned.1.call-update) | async-done | bytes 1048592 | tf_op jit(solution)/shard_map/all_gather | solution.py:29
  72.5 39.5 %all-gather.21.cloned.1.call-done = bf16[1,2048,256]{2,1,0:T(8,128)(2,1)} async-done(((bf16[1,256,256]{2,1,0:T(8,128)(2,1)}), bf16[1,2048,256]{2,1,0:T(8,128)(2,1)}) %all-gather.21.cloned.1.call-update) | async-done | bytes 1048592 | tf_op jit(solution)/shard_map/all_gather | solution.py:30
  113.7 2.5 collective-permute-start
  118.1 4.8 %fusion.45 = (f32[256]{0:T(256)S(1)}, f32[1,256,256]{2,0,1:T(1,128)S(1)}) fusion(f32[1,128,256]{2,1,0:T(8,128)S(1)} %get-tuple-element.6, bf16[1,383,256]{2,1,0:T(8,128)(2,1)S(1)} %maximum_bitcast_fusion), kind=kOutput, calls=%fused_computation.71 | convolution fusion | flops 100728576 | bytes 590336 | tf_op jit(solution)/shard_map/conv_general_dilated | solution.py:37
  123.0 5.7 %psum.28 = f32[256,1]{0,1:T(1,128)S(1)} all-reduce(f32[256,1]{0,1:T(1,128)S(1)} %bitcast.98), channel_id=1, replica_groups=mesh['sp'=8,'tp'=4] {'tp'}, use_global_device_ids=true, to_apply=%region_2.0 | all-reduce | flops 256 | bytes 2048 | tf_op jit(solution)/shard_map/psum | solution.py:46
  128.8 7.0 %psum.29 = f32[256,1]{0,1:T(1,128)S(1)} all-reduce(f32[256,1]{0,1:T(1,128)S(1)} %bitcast.94), channel_id=1, replica_groups=mesh['sp'=8,'tp'=4] {'tp'}, use_global_device_ids=true, to_apply=%region_4.0 | all-reduce | flops 256 | bytes 2048 | tf_op jit(solution)/shard_map/psum | solution.py:48
  135.8 16.2 %all-gather.23.cloned.1.call-done = bf16[1,256,2048]{2,1,0:T(8,128)(2,1)} async-done(((bf16[1,256,256]{2,1,0:T(8,128)(2,1)}), bf16[1,256,2048]{2,1,0:T(8,128)(2,1)}) %all-gather.23.cloned.1.call-update) | async-done | bytes 1048592 | tf_op jit(solution)/shard_map/all_gather | solution.py:52
  152.0 3.1 fusion.20
  155.2 30.3 %reduce-scatter.3.cloned.1.call-done = f32[256,512]{1,0:T(8,128)} async-done(((f32[256,2048]{1,0:T(8,128)}), f32[256,512]{1,0:T(8,128)}) %reduce-scatter.3.cloned.1.call-update) | async-done | bytes 524304 | tf_op jit(solution)/shard_map/reduce_scatter | solution.py:54
  189.6 14.6 %all-gather.25.cloned.1.call-done = bf16[1024,512]{1,0:T(8,128)(2,1)} async-done(((bf16[256,512]{1,0:T(8,128)(2,1)}), bf16[1024,512]{1,0:T(8,128)(2,1)}) %all-gather.25.cloned.1.call-update) | async-done | bytes 1048592 | tf_op jit(solution)/shard_map/all_gather | solution.py:22
  204.1 2.8 bitcast_convert_fusion
  207.0 2.0 copy.20
  209.7 36.9 %all-gather.27.cloned.1.call-done = bf16[1,2048,256]{2,1,0:T(8,128)(2,1)} async-done(((bf16[1,256,256]{2,1,0:T(8,128)(2,1)}), bf16[1,2048,256]{2,1,0:T(8,128)(2,1)}) %all-gather.27.cloned.1.call-update) | async-done | bytes 1048592 | tf_op jit(solution)/shard_map/all_gather | solution.py:29
  248.3 39.4 %all-gather.29.cloned.1.call-done = bf16[1,2048,256]{2,1,0:T(8,128)(2,1)} async-done(((bf16[1,256,256]{2,1,0:T(8,128)(2,1)}), bf16[1,2048,256]{2,1,0:T(8,128)(2,1)}) %all-gather.29.cloned.1.call-update) | async-done | bytes 1048592 | tf_op jit(solution)/shard_map/all_gather | solution.py:30
  289.5 2.5 collective-permute-start.1
  293.9 4.8 %fusion.46 = (f32[256]{0:T(256)S(1)}, f32[1,256,256]{2,0,1:T(1,128)S(1)}) fusion(f32[1,128,256]{2,1,0:T(8,128)S(1)} %get-tuple-element.5, bf16[1,383,256]{2,1,0:T(8,128)(2,1)S(1)} %maximum_bitcast_fusion.1), kind=kOutput, calls=%fused_computation.72 | convolution fusion | flops 100728576 | bytes 590336 | tf_op jit(solution)/shard_map/conv_general_dilated | solution.py:37
  298.7 5.7 %psum.30 = f32[256,1]{0,1:T(1,128)S(1)} all-reduce(f32[256,1]{0,1:T(1,128)S(1)} %bitcast.99), channel_id=1, replica_groups=mesh['sp'=8,'tp'=4] {'tp'}, use_global_device_ids=true, to_apply=%region_8.9 | all-reduce | flops 256 | bytes 2048 | tf_op jit(solution)/shard_map/psum | solution.py:46
  304.6 7.0 %psum.31 = f32[256,1]{0,1:T(1,128)S(1)} all-reduce(f32[256,1]{0,1:T(1,128)S(1)} %bitcast.95), channel_id=1, replica_groups=mesh['sp'=8,'tp'=4] {'tp'}, use_global_device_ids=true, to_apply=%region_10.11 | all-reduce | flops 256 | bytes 2048 | tf_op jit(solution)/shard_map/psum | solution.py:48
  311.6 16.3 %all-gather.31.cloned.1.call-done = bf16[1,256,2048]{2,1,0:T(8,128)(2,1)} async-done(((bf16[1,256,256]{2,1,0:T(8,128)(2,1)}), bf16[1,256,2048]{2,1,0:T(8,128)(2,1)}) %all-gather.31.cloned.1.call-update) | async-done | bytes 1048592 | tf_op jit(solution)/shard_map/all_gather | solution.py:52
  327.9 3.1 fusion.15
  331.0 30.3 %reduce-scatter.5.cloned.1.call-done = f32[256,512]{1,0:T(8,128)} async-done(((f32[256,2048]{1,0:T(8,128)}), f32[256,512]{1,0:T(8,128)}) %reduce-scatter.5.cloned.1.call-update) | async-done | bytes 524304 | tf_op jit(solution)/shard_map/reduce_scatter | solution.py:54
  (66 shorter events, 24.4 us)
Async XLA Ops:
  6.5 6.1 %copy-start.5 = (f32[2,2048]{1,0:T(2,128)S(1)}, f32[2,2048]{1,0:T(2,128)}, u32[]{:S(2)}) copy-start(f32[2,2048]{1,0:T(2,128)} %param.8) | copy-start | bytes 49156
  6.5 6.1 %copy-start.4 = (f32[2,128,256]{2,1,0:T(8,128)S(1)}, f32[2,128,256]{2,1,0:T(8,128)}, u32[]{:S(2)}) copy-start(f32[2,128,256]{2,1,0:T(8,128)} %param.11) | copy-start | bytes 786436
  6.5 21.8 %all-gather.17.cloned.1.call-start = ((), (), s32[]{:S(2)}) async-start(), calls=%async_computation.4 | async-start | bytes 1310720 | tf_op jit(solution)/shard_map/all_gather | solution.py:22
  7.3 63.5 %all-gather.19.cloned.1.call-start = ((), (), s32[]{:S(2)}) async-start(), calls=%async_computation.5 | async-start | bytes 1179648 | tf_op jit(solution)/shard_map/all_gather | solution.py:29
  9.0 102.9 %all-gather.21.cloned.1.call-start = ((), (), s32[]{:S(2)}) async-start(), calls=%async_computation.6 | async-start | bytes 1179648 | tf_op jit(solution)/shard_map/all_gather | solution.py:30
  10.8 141.2 %all-gather.23.cloned.1.call-start = ((), (), s32[]{:S(2)}) async-start(), calls=%async_computation.7 | async-start | bytes 1179648 | tf_op jit(solution)/shard_map/all_gather | solution.py:52
  12.5 172.9 %reduce-scatter.3.cloned.1.call-start = ((), (), s32[]{:S(2)}) async-start(), calls=%async_computation.2 | async-start | bytes 2621440 | tf_op jit(solution)/shard_map/reduce_scatter | solution.py:54
  31.2 2.0 copy-start
  33.9 82.3 %copy-start.6 = (f32[2,256]{1,0:T(2,128)S(1)}, f32[2,256]{1,0:T(2,128)}, u32[]{:S(2)}) copy-start(f32[2,256]{1,0:T(2,128)} %param.12) | copy-start | bytes 6148
  113.7 4.4 %collective-permute-start = (bf16[128,256]{1,0:T(8,128)(2,1)S(1)}, bf16[128,256]{1,0:T(8,128)(2,1)S(1)}, u32[]{:S(2)}, u32[]{:S(2)}) collective-permute-start(bf16[128,256]{1,0:T(8,128)(2,1)S(1)} %slice.64), channel_id=1, source_target_pairs={{0,4},{4,8},{8,12},{12,16},{16,20},{20,24},{24,28},{1,5},{5,9},{9,... | collective-permute-start | bytes 196616 | tf_op jit(solution)/shard_map/ppermute | solution.py:13
  152.0 33.5 %copy-start.3 = (bf16[256,512]{1,0:T(8,128)(2,1)S(1)}, bf16[256,512]{1,0:T(8,128)(2,1)}, u32[]{:S(2)}) copy-start(bf16[256,512]{1,0:T(8,128)(2,1)} %param.7) | copy-start | bytes 786436
  155.1 49.0 %all-gather.25.cloned.1.call-start = ((), (), s32[]{:S(2)}) async-start(), calls=%async_computation.8 | async-start | bytes 1310720 | tf_op jit(solution)/shard_map/all_gather | solution.py:22
  187.3 59.3 %all-gather.27.cloned.1.call-start = ((), (), s32[]{:S(2)}) async-start(), calls=%async_computation.9 | async-start | bytes 1179648 | tf_op jit(solution)/shard_map/all_gather | solution.py:29
  188.0 99.7 %all-gather.29.cloned.1.call-start = ((), (), s32[]{:S(2)}) async-start(), calls=%async_computation.10 | async-start | bytes 1179648 | tf_op jit(solution)/shard_map/all_gather | solution.py:30
  188.8 139.1 %all-gather.31.cloned.1.call-start = ((), (), s32[]{:S(2)}) async-start(), calls=%async_computation.11 | async-start | bytes 1179648 | tf_op jit(solution)/shard_map/all_gather | solution.py:52
  189.5 171.9 %reduce-scatter.5.cloned.1.call-start = ((), (), s32[]{:S(2)}) async-start(), calls=%async_computation.3 | async-start | bytes 2621440 | tf_op jit(solution)/shard_map/reduce_scatter | solution.py:54
  207.0 2.0 copy-start.1
  289.5 4.4 %collective-permute-start.1 = (bf16[128,256]{1,0:T(8,128)(2,1)S(1)}, bf16[128,256]{1,0:T(8,128)(2,1)S(1)}, u32[]{:S(2)}, u32[]{:S(2)}) collective-permute-start(bf16[128,256]{1,0:T(8,128)(2,1)S(1)} %slice.66), channel_id=1, source_target_pairs={{0,4},{4,8},{8,12},{12,16},{16,20},{20,24},{24,28},{1,5},{5,9},{9,... | collective-permute-start | bytes 196616 | tf_op jit(solution)/shard_map/ppermute | solution.py:13
  327.9 33.5 %copy-start.2 = (bf16[256,512]{1,0:T(8,128)(2,1)S(1)}, bf16[256,512]{1,0:T(8,128)(2,1)}, u32[]{:S(2)}) copy-start(bf16[256,512]{1,0:T(8,128)(2,1)} %add_convert_fusion.1) | copy-start | bytes 786436
Sparse Core Ops, SparseCore 0:
  8.9 19.4 all-gather.16
  30.5 40.2 all-gather.18
  72.9 38.9 all-gather.20
  113.8 38.0 all-gather.22
  155.2 30.1 reduce-scatter.2
  187.4 16.6 all-gather.24
  206.3 40.2 all-gather.26
  248.7 38.9 all-gather.28
  289.8 38.0 all-gather.30
  331.2 30.1 reduce-scatter.4
